TPU v7x, 32 devices: a whole 2x2x4 slice. The times are simulated.
32 devices in a mesh: ep: 8 (over z, y), tp: 4 (over x, core).
Axes of the slice: x: 2, y: 2, z: 4, core: 2. Of those that a mesh axis runs over, the one named last changes fastest.
Arguments:
- resid: bfloat16 [256, 2048], P('ep'), may hold values from -6 to 6
- mix_gain: bfloat16 [2048], replicated, may hold values from 0.099609375 to 1.8984375
- proj_x: bfloat16 [2048, 512], P(None, 'tp'), may hold values from -0.125 to 0.125
- proj_z: bfloat16 [2048, 512], P(None, 'tp'), may hold values from -0.125 to 0.125
- proj_b: bfloat16 [2048, 512], P(None, 'tp'), may hold values from -0.125 to 0.125
- proj_c: bfloat16 [2048, 512], P(None, 'tp'), may hold values from -0.125 to 0.125
- proj_step: bfloat16 [2048, 8], replicated, may hold values from -0.125 to 0.125
- step_bias: float32 [8], P('tp'), may hold values from -5 to -1
- decay_rate: float32 [8], P('tp'), may hold values from 1 to 16
- conv_taps: bfloat16 [3, 4, 512], P(None, None, 'tp'), may hold values from -3 to 3
- conv_state: bfloat16 [256, 3, 3, 512], P('ep', None, None, 'tp'), may hold values from -6 to 6
- scan_state: float32 [256, 8, 64, 128], P('ep', 'tp'), may hold values from -2.5 to 2.5
- inner_gain: bfloat16 [512], P('tp'), may hold values from 0.099609375 to 1.8984375
- proj_out: bfloat16 [512, 2048], P('tp'), may hold values from -0.25 to 0.25
- post_gain: bfloat16 [2048], replicated, may hold values from 0.099609375 to 1.8984375
- ffn_gain: bfloat16 [2048], replicated, may hold values from 0.099609375 to 1.8984375
- group_router: bfloat16 [2048, 2], replicated, may hold values from -0.125 to 0.125
- expert_router: bfloat16 [2048, 8], replicated, may hold values from -0.125 to 0.125
- route_experts: int32 [256, 4], P('ep'), may hold values from 0 to 7, as said below
- expert_gate: bfloat16 [8, 2048, 1024], P('ep', None, 'tp'), may hold values from -0.125 to 0.125
- expert_up: bfloat16 [8, 2048, 1024], P('ep', None, 'tp'), may hold values from -0.125 to 0.125
- expert_down: bfloat16 [8, 1024, 2048], P('ep', 'tp')
- dense_switch: bfloat16 [2048], replicated, may hold values from -0.125 to 0.125
- dense_gate: bfloat16 [2048, 2048], P('ep', 'tp'), may hold values from -0.125 to 0.125
- dense_up: bfloat16 [2048, 2048], P('ep', 'tp'), may hold values from -0.125 to 0.125
- dense_down: bfloat16 [2048, 2048], P('ep', 'tp')
- out_gain: bfloat16 [2048], P('tp'), may hold values from 0.099609375 to 1.8984375
Outputs:
- layer_out: bfloat16 [256, 2048], P('ep', 'tp')
- new_state: float32 [256, 8, 64, 128], P('ep', 'tp')
- new_conv: bfloat16 [256, 3, 3, 512], P('ep', None, None, 'tp')
Inputs may be any that keep to these rules, and one draw needn't show every extreme that they name: `route_experts`: each row names 4 different experts, all from one group of 4 consecutive expert numbers. Within each aligned block of 32 rows (the rows of one index of ep) no expert is named more than 32 times, and one expert, the same in every block, is named exactly 32 times in every block.
All inputs are finite; a program needn't handle non-finite values.
Results may differ from a plain program's by a relative error of at most 0.019.
Values may be sent and summed in bfloat16 or wider, within the bound.
A program may use at most 64 MiB of HBM per device.

v0:
```python
import jax
import jax.numpy as jnp
from jax import lax
from jax.sharding import PartitionSpec as P

norm_eps = 1e-06


def scaled_rows(values, gain):
    values = values.astype(jnp.float32)
    mean_square = jnp.mean(values * values, axis=-1, keepdims=True)
    return values * lax.rsqrt(mean_square + norm_eps) * gain.astype(jnp.float32)


def softmax_plain(logits):
    weights = jnp.exp(logits)
    return weights / jnp.sum(weights, axis=-1, keepdims=True)


def on_device(
    resid,
    mix_gain,
    proj_x,
    proj_z,
    proj_b,
    proj_c,
    proj_step,
    step_bias,
    decay_rate,
    conv_taps,
    conv_state,
    scan_state,
    inner_gain,
    proj_out,
    post_gain,
    ffn_gain,
    group_router,
    expert_router,
    route_experts,
    expert_gate,
    expert_up,
    expert_down,
    dense_switch,
    dense_gate,
    dense_up,
    dense_down,
    out_gain,
):
    tp_index = lax.axis_index("tp")
    seqs = resid.shape[0]
    width = resid.shape[1]
    quarter = width // lax.axis_size("tp")
    heads_here = scan_state.shape[1]
    head_dim = scan_state.shape[2]
    state_dim = scan_state.shape[3]
    channels = conv_state.shape[3]
    repeat = heads_here // (channels // state_dim)
    normed = scaled_rows(resid, mix_gain).astype(jnp.bfloat16)
    fresh = jnp.stack(
        [
            jnp.dot(normed, proj_x, preferred_element_type=jnp.float32),
            jnp.dot(normed, proj_b, preferred_element_type=jnp.float32),
            jnp.dot(normed, proj_c, preferred_element_type=jnp.float32),
        ],
        axis=1,
    ).astype(jnp.bfloat16)
    gate_z = jnp.dot(normed, proj_z, preferred_element_type=jnp.float32)
    step_all = jnp.dot(normed, proj_step, preferred_element_type=jnp.float32)
    step_raw = lax.dynamic_slice_in_dim(step_all, tp_index * heads_here, heads_here, 1)
    history = jnp.concatenate([conv_state, fresh[:, :, None, :]], axis=2)
    activated = jax.nn.silu(
        jnp.sum(history.astype(jnp.float32) * conv_taps.astype(jnp.float32)[None], axis=2)
    )
    xs_heads = activated[:, 0].reshape(seqs, heads_here, head_dim)
    b_heads = jnp.repeat(activated[:, 1].reshape(seqs, -1, state_dim), repeat, axis=1)
    c_heads = jnp.repeat(activated[:, 2].reshape(seqs, -1, state_dim), repeat, axis=1)
    step = jax.nn.softplus(step_raw + step_bias)
    keep = jnp.exp(-decay_rate * step)
    driven = step[:, :, None] * xs_heads
    new_state = keep[:, :, None, None] * scan_state + driven[:, :, :, None] * b_heads[:, :, None, :]
    read = jnp.sum(new_state * c_heads[:, :, None, :], axis=3).reshape(seqs, channels)
    gated = (read * jax.nn.silu(gate_z) * inner_gain.astype(jnp.float32)).astype(jnp.bfloat16)
    mixed = lax.psum(
        jnp.dot(gated, proj_out, preferred_element_type=jnp.float32).astype(jnp.bfloat16), "tp"
    ).astype(jnp.float32)
    stream = (resid.astype(jnp.float32) + scaled_rows(mixed, post_gain)).astype(jnp.bfloat16)
    feed = scaled_rows(stream, ffn_gain).astype(jnp.bfloat16)
    feed_quarter = lax.dynamic_slice_in_dim(feed, tp_index * quarter, quarter, 1)
    expert_count = expert_router.shape[1]
    group_size = expert_count // group_router.shape[1]
    pick_count = route_experts.shape[1]
    group_prob = softmax_plain(jnp.dot(feed, group_router, preferred_element_type=jnp.float32))
    expert_logits = jnp.dot(feed, expert_router, preferred_element_type=jnp.float32)
    matches = route_experts[:, :, None] == jnp.arange(expert_count, dtype=jnp.int32)[None, None, :]
    pick_logits = jnp.sum(jnp.where(matches, expert_logits[:, None, :], 0.0), axis=2)
    chosen_group = route_experts[:, 0] // group_size
    group_ids = jnp.arange(group_router.shape[1], dtype=jnp.int32)
    group_weight = jnp.sum(
        jnp.where(chosen_group[:, None] == group_ids[None, :], group_prob, 0.0), axis=1
    )
    pick_weight = softmax_plain(pick_logits) * group_weight[:, None]
    capacity = 2 * seqs * pick_count // expert_count
    flat_picks = route_experts.reshape(-1)
    one_hot = (flat_picks[:, None] == jnp.arange(expert_count, dtype=jnp.int32)[None, :]).astype(
        jnp.int32
    )
    slot = jnp.sum((jnp.cumsum(one_hot, axis=0) - one_hot) * one_hot, axis=1)
    target = flat_picks * capacity + slot
    repeated = jnp.repeat(feed, pick_count, axis=0)
    outgoing = jnp.zeros((expert_count * capacity, width), jnp.bfloat16).at[target].set(repeated)
    outgoing = outgoing.reshape(expert_count, capacity, width)
    arrived = lax.all_to_all(outgoing, "ep", split_axis=0, concat_axis=0, tiled=True)
    sources = arrived.shape[0]
    items = arrived.shape[1]
    rows = arrived.reshape(sources * items, width)
    gate_value = jnp.dot(rows, expert_gate[0], preferred_element_type=jnp.float32)
    up_value = jnp.dot(rows, expert_up[0], preferred_element_type=jnp.float32)
    hidden = (jax.nn.silu(gate_value) * up_value).astype(jnp.bfloat16)
    result = jnp.dot(hidden, expert_down[0], preferred_element_type=jnp.float32).reshape(
        sources, items, width
    )
    summed = lax.psum_scatter(result.astype(jnp.bfloat16), "tp", scatter_dimension=2, tiled=True)
    returned = lax.all_to_all(summed, "ep", split_axis=0, concat_axis=0, tiled=True)
    fetched = returned.reshape(expert_count * capacity, quarter)[target].reshape(
        seqs, pick_count, quarter
    )
    routed = jnp.sum(fetched.astype(jnp.float32) * pick_weight[:, :, None], axis=1)
    gate_piece = jnp.einsum(
        "sd,cd->sc",
        feed_quarter,
        lax.all_gather(dense_gate, "ep", axis=0, tiled=True),
        preferred_element_type=jnp.float32,
    )
    up_piece = jnp.einsum(
        "sd,cd->sc",
        feed_quarter,
        lax.all_gather(dense_up, "ep", axis=0, tiled=True),
        preferred_element_type=jnp.float32,
    )
    gate_sum = gate_piece
    up_sum = up_piece
    gate_sum, up_sum = (
        lax.psum(gate_sum.astype(jnp.bfloat16), "tp").astype(jnp.float32),
        lax.psum(up_sum.astype(jnp.bfloat16), "tp").astype(jnp.float32),
    )
    dense_hidden = (jax.nn.silu(gate_sum) * up_sum).astype(jnp.bfloat16)
    dense_out = jnp.dot(
        dense_hidden,
        lax.all_gather(dense_down, "ep", axis=0, tiled=True),
        preferred_element_type=jnp.float32,
    )
    switch = jax.nn.sigmoid(jnp.dot(feed, dense_switch, preferred_element_type=jnp.float32))
    combined = routed + switch[:, None] * dense_out
    total_square = lax.psum(jnp.sum(combined * combined, axis=1), "tp")
    scale = lax.rsqrt(total_square / width + norm_eps)
    stream_part = lax.dynamic_slice_in_dim(stream, tp_index * quarter, quarter, 1).astype(
        jnp.float32
    )
    layer_out = (stream_part + combined * scale[:, None] * out_gain.astype(jnp.float32)).astype(
        jnp.bfloat16
    )
    new_conv = history[:, :, 1:, :]
    return (layer_out, new_state, new_conv)


def solution(mesh):
    placed = (
        P("ep", None),
        P(),
        P(None, "tp"),
        P(None, "tp"),
        P(None, "tp"),
        P(None, "tp"),
        P(),
        P("tp"),
        P("tp"),
        P(None, None, "tp"),
        P("ep", None, None, "tp"),
        P("ep", "tp", None, None),
        P("tp"),
        P("tp", None),
        P(),
        P(),
        P(),
        P(),
        P("ep", None),
        P("ep", None, "tp"),
        P("ep", None, "tp"),
        P("ep", "tp", None),
        P(),
        P("ep", "tp"),
        P("ep", "tp"),
        P("ep", "tp"),
        P("tp"),
    )
    return jax.shard_map(
        on_device,
        mesh=mesh,
        in_specs=placed,
        out_specs=(P("ep", "tp"), P("ep", "tp", None, None), P("ep", None, None, "tp")),
        check_vma=False,
    )
```

profile of v0, /device:TPU:0, one launch (start us, length us, event | category | flops | bytes accessed | tf_op | source)
XLA Modules:
  0.0 219.6 jit_solution(17043526989973223200)
XLA Ops:
  8.1 0.8 convert_element_type.91
  9.0 1.1 fusion.24
  10.1 1.4 fusion.2
  11.4 1.4 fusion.3
  12.8 1.4 fusion.4
  14.2 0.9 multiply_reduce_fusion.2
  15.3 1.0 fusion.48
  16.6 0.1 broadcast_multiply_fusion
  16.7 2.1 multiply_reduce_fusion
  18.8 0.1 reshape.185
  18.9 2.3 %convolution_convert_fusion.3 = bf16[32,2048]{1,0:T(8,128)(2,1)} fusion(bf16[128,2048]{1,0:T(8,128)(2,1)} %param.40, f32[32,128]{1,0:T(8,128)S(1)} %reshape.185, f32[128]{0:T(128)S(1)} %convert_element_type.95, bf16[2048,128]{1,0:T(8,128)(2,1)} %param.30, bf16[32,2048]{1,0:T(8,128)(2,1)S(1)} %copy-done.1, f32[2048]{0:T(1024)S(1)} %convert_element_type.91, ...), kind=kOutput, calls=%fused_computation.5 | convolution fusion | flops 33910784 | bytes 1335936 | tf_op jit(solution)/shard_map/dot_general | solution.py:84
  21.3 0.5 all-gather.6.cloned.1.call-update
  21.9 0.1 copy.45
  22.0 0.1 eq.43
  22.2 0.1 fusion.31
  22.2 0.2 reduce_window_sum.11
  22.4 0.2 select_reduce_fusion
  22.6 0.1 copy.44
  22.7 0.1 mul.252
  22.8 33.1 %all-reduce.4.cloned.1.call-done = bf16[32,2048]{1,0:T(8,128)(2,1)} async-done(((bf16[32,2048]{1,0:T(8,128)(2,1)}), bf16[32,2048]{1,0:T(8,128)(2,1)}) %all-reduce.4.cloned.1.call-update) | async-done | bytes 131088 | tf_op jit(solution)/shard_map/psum | solution.py:83
  55.9 1.0 fusion.15
  57.0 1.2 fusion.17
  58.2 0.1 fusion.19
  58.3 0.2 broadcast_in_dim.14
  58.5 0.9 reshape.203
  59.4 2.2 %scatter_custom_fusion = bf16[256,2048]{1,0:T(8,128)(2,1)S(1)} fusion(s32[128]{0:T(128)S(1)} %fusion.39, bf16[128,2048]{1,0:T(8,128)(2,1)} %reshape.203, bf16[]{:T(256)} %constant.57.clone.1), kind=kCustom, calls=%fused_computation.28 | custom fusion | bytes 1049088 | tf_op jit(solution)/shard_map/scatter | solution.py:110
  61.7 36.1 %all_to_all.10 = bf16[8,32,2048]{2,1,0:T(8,128)(2,1)S(1)} all-to-all(bf16[8,32,2048]{2,1,0:T(8,128)(2,1)S(1)} %bitcast.63), channel_id=1, replica_groups=mesh['ep'=8,'tp'=4] {'ep'}, dimensions={0} | all-to-all | bytes 2097152 | tf_op jit(solution)/shard_map/all_to_all | solution.py:112
  97.7 0.4 fusion.11
  98.2 0.4 fusion
  98.7 1.4 convolution_convert_fusion
  100.2 0.5 all-gather.4.cloned.1.call-update
  100.8 0.5 all-gather.8.cloned.1.call-update
  101.4 0.6 slice.31
  102.0 0.1 fusion.57
  102.2 0.2 fusion.56
  102.4 0.1 fusion.8
  102.6 3.1 %convolution_convert_fusion.1 = bf16[32,2048]{1,0:T(8,128)(2,1)} fusion(bf16[2048,512]{1,0:T(8,128)(2,1)} %all-gather.6.cloned.1.call-done, bf16[32,2048]{1,0:T(8,128)(2,1)S(1)} %fusion.19, s32[]{:T(128)S(6)} %select_n.38), kind=kOutput, calls=%fused_computation.3 | convolution fusion | flops 67174400 | bytes 2260996 | tf_op jit(solution)/shard_map/sd,cd->sc/dot_general | solution.py:134
  105.7 17.5 %reduce-scatter.2.cloned.1.call-done = bf16[8,32,512]{2,1,0:T(8,128)(2,1)} async-done(((bf16[8,32,2048]{2,1,0:T(8,128)(2,1)}), bf16[8,32,512]{2,1,0:T(8,128)(2,1)}) %reduce-scatter.2.cloned.1.call-update) | async-done | bytes 262160 | tf_op jit(solution)/shard_map/reduce_scatter | solution.py:122
  123.2 5.5 %all-to-all-start.1 = ((bf16[8,32,512]{2,1,0:T(8,128)(2,1)}), bf16[8,32,512]{2,1,0:T(8,128)(2,1)S(1)}, u32[]{:S(2)}, u32[]{:S(2)}) async-start(bf16[8,32,512]{2,1,0:T(8,128)(2,1)} %reduce-scatter.2.cloned.1.call-done), calls=%async_computation.2 | async-start | bytes 524288 | tf_op jit(solution)/shard_map/all_to_all | solution.py:123
  128.8 24.4 %all-gather.4.cloned.1.call-done = bf16[2048,512]{1,0:T(8,128)(2,1)} async-done(((bf16[256,512]{1,0:T(8,128)(2,1)}), bf16[2048,512]{1,0:T(8,128)(2,1)}) %all-gather.4.cloned.1.call-update) | async-done | bytes 2097168 | tf_op jit(solution)/shard_map/all_gather | solution.py:131
  153.2 3.0 %convolution_convert_fusion.2 = bf16[32,2048]{1,0:T(8,128)(2,1)} fusion(bf16[2048,512]{1,0:T(8,128)(2,1)} %all-gather.4.cloned.1.call-done, bf16[32,2048]{1,0:T(8,128)(2,1)S(1)} %fusion.19, s32[]{:T(128)S(6)} %select_n.38), kind=kOutput, calls=%fused_computation.4 | convolution fusion | flops 67174400 | bytes 2260996 | tf_op jit(solution)/shard_map/sd,cd->sc/dot_general | solution.py:128
  156.3 0.8 gather_fusion
  157.2 0.1 reshape.190
  157.3 0.2 multiply_reduce_fusion.1
  157.5 46.1 %all-gather.8.cloned.1.call-done = bf16[2048,512]{1,0:T(8,128)(2,1)} async-done(((bf16[256,512]{1,0:T(8,128)(2,1)}), bf16[2048,512]{1,0:T(8,128)(2,1)}) %all-gather.8.cloned.1.call-update) | async-done | bytes 2097168 | tf_op jit(solution)/shard_map/all_gather | solution.py:149
  203.6 2.3 %multiply_reduce_fusion.3 = (f32[32]{0:T(128)S(1)}, f32[32,512]{1,0:T(8,128)S(1)}) fusion(f32[32,512]{1,0:T(8,128)S(1)} %multiply_reduce_fusion.1, bf16[2048,512]{1,0:T(8,128)(2,1)} %all-gather.8.cloned.1.call-done, bf16[32,2048]{1,0:T(8,128)(2,1)} %get-tuple-element.3, bf16[32,2048]{1,0:T(8,128)(2,1)} %get-tuple-element.4, f32[32]{0:T(128)S(1)} %fusion.8), kind=kOutput, calls=%fused_computation.58 | convolution fusion | flops 67698656 | bytes 2490624 | tf_op jit(solution)/shard_map/dot_general | solution.py:147
  205.9 5.7 %psum.31 = f32[32]{0:T(128)S(1)} all-reduce(f32[32]{0:T(128)S(1)} %get-tuple-element.18), channel_id=1, replica_groups=mesh['ep'=8,'tp'=4] {'tp'}, use_global_device_ids=true, to_apply=%region_18.19 | all-reduce | flops 32 | bytes 256 | tf_op jit(solution)/shard_map/psum | solution.py:154
  211.5 0.7 add_convert_fusion
  (70 shorter events, 1.0 us)
Async XLA Ops:
  8.0 90.7 %copy-start = (bf16[1,256,2048]{2,1,0:T(8,128)(2,1)S(1)}, bf16[1,256,2048]{2,1,0:T(8,128)(2,1)}, u32[]{:S(2)}) copy-start(bf16[1,256,2048]{2,1,0:T(8,128)(2,1)} %param.48) | copy-start | bytes 3145732
  8.0 7.3 %copy-start.1 = (bf16[32,2048]{1,0:T(8,128)(2,1)S(1)}, bf16[32,2048]{1,0:T(8,128)(2,1)}, u32[]{:S(2)}) copy-start(bf16[32,2048]{1,0:T(8,128)(2,1)} %param.27) | copy-start | bytes 393220
  8.0 6.2 %copy-start.9 = (bf16[3,4,128]{2,1,0:T(4,128)(2,1)S(1)}, bf16[3,4,128]{2,1,0:T(4,128)(2,1)}, u32[]{:S(2)}) copy-start(bf16[3,4,128]{2,1,0:T(4,128)(2,1)} %param.36) | copy-start | bytes 9220
  8.0 8.2 %copy-start.14 = (f32[2]{0:T(128)S(1)}, f32[2]{0:T(128)}, u32[]{:S(2)}) copy-start(f32[2]{0:T(128)} %param.35) | copy-start | bytes 28
  8.0 8.2 %copy-start.11 = (f32[2]{0:T(128)S(1)}, f32[2]{0:T(128)}, u32[]{:S(2)}) copy-start(f32[2]{0:T(128)} %param.34) | copy-start | bytes 28
  8.1 8.6 %copy-start.2 = (f32[32,2,64,128]{3,2,1,0:T(8,128)S(1)}, f32[32,2,64,128]{3,2,1,0:T(8,128)}, u32[]{:S(2)}) copy-start(f32[32,2,64,128]{3,2,1,0:T(8,128)} %param.38) | copy-start | bytes 6291460
  8.1 47.9 %all-reduce.4.cloned.1.call-start = ((), (), s32[]{:S(2)}) async-start(), calls=%async_computation.3 | async-start | bytes 262144 | tf_op jit(solution)/shard_map/psum | solution.py:83
  16.7 2.2 %copy-start.15 = (bf16[128]{0:T(256)(128)(2,1)S(1)}, bf16[128]{0:T(256)(128)(2,1)}, u32[]{:S(2)}) copy-start(bf16[128]{0:T(256)(128)(2,1)} %param.39) | copy-start | bytes 772
  16.7 5.2 %copy-start.5 = (s32[32,4]{0,1:T(4,128)S(1)}, s32[32,4]{0,1:T(4,128)}, u32[]{:S(2)}) copy-start(s32[32,4]{0,1:T(4,128)} %param.45) | copy-start | bytes 1540
  16.7 5.3 %copy-start.6 = (bf16[2048]{0:T(1024)(128)(2,1)S(1)}, bf16[2048]{0:T(1024)(128)(2,1)}, u32[]{:S(2)}) copy-start(bf16[2048]{0:T(1024)(128)(2,1)} %param.41) | copy-start | bytes 12292
  16.7 5.3 %copy-start.7 = (bf16[2048]{0:T(1024)(128)(2,1)S(1)}, bf16[2048]{0:T(1024)(128)(2,1)}, u32[]{:S(2)}) copy-start(bf16[2048]{0:T(1024)(128)(2,1)} %param.42) | copy-start | bytes 12292
  21.3 81.3 %all-gather.6.cloned.1.call-start = ((), (), s32[]{:S(2)}) async-start(), calls=%async_computation.6 | async-start | bytes 2359296 | tf_op jit(solution)/shard_map/all_gather | solution.py:137
  21.9 101.4 %reduce-scatter.2.cloned.1.call-start = ((), (), s32[]{:S(2)}) async-start(), calls=%async_computation.4 | async-start | bytes 1310720 | tf_op jit(solution)/shard_map/reduce_scatter | solution.py:122
  58.5 39.2 %copy-start.3 = (bf16[1,2048,256]{2,1,0:T(8,128)(2,1)S(1)}, bf16[1,2048,256]{2,1,0:T(8,128)(2,1)}, u32[]{:S(2)}) copy-start(bf16[1,2048,256]{2,1,0:T(8,128)(2,1)} %param.46) | copy-start | bytes 3145732
  61.6 36.5 %copy-start.12 = (bf16[1,2048,256]{2,1,0:T(8,128)(2,1)S(1)}, bf16[1,2048,256]{2,1,0:T(8,128)(2,1)}, u32[]{:S(2)}) copy-start(bf16[1,2048,256]{2,1,0:T(8,128)(2,1)} %param.47) | copy-start | bytes 3145732
  98.6 2.7 %copy-start.8 = (bf16[2048]{0:T(1024)(128)(2,1)S(1)}, bf16[2048]{0:T(1024)(128)(2,1)}, u32[]{:S(2)}) copy-start(bf16[2048]{0:T(1024)(128)(2,1)} %param.49) | copy-start | bytes 12292
  98.6 2.7 %copy-start.10 = (bf16[512]{0:T(512)(128)(2,1)S(1)}, bf16[512]{0:T(512)(128)(2,1)}, u32[]{:S(2)}) copy-start(bf16[512]{0:T(512)(128)(2,1)} %param.53) | copy-start | bytes 3076
  98.7 3.4 %copy-start.4 = (bf16[2048,8]{0,1:T(8,128)(2,1)S(1)}, bf16[2048,8]{0,1:T(8,128)(2,1)}, u32[]{:S(2)}) copy-start(bf16[2048,8]{0,1:T(8,128)(2,1)} %param.44) | copy-start | bytes 98308
  98.7 3.6 %copy-start.13 = (bf16[2048,2]{0,1:T(2,128)(2,1)S(1)}, bf16[2048,2]{0,1:T(2,128)(2,1)}, u32[]{:S(2)}) copy-start(bf16[2048,2]{0,1:T(2,128)(2,1)} %param.43) | copy-start | bytes 24580
  100.2 53.1 %all-gather.4.cloned.1.call-start = ((), (), s32[]{:S(2)}) async-start(), calls=%async_computation.5 | async-start | bytes 2359296 | tf_op jit(solution)/shard_map/all_gather | solution.py:131
  100.7 102.8 %all-gather.8.cloned.1.call-start = ((), (), s32[]{:S(2)}) async-start(), calls=%async_computation.7 | async-start | bytes 2359296 | tf_op jit(solution)/shard_map/all_gather | solution.py:149
  123.2 33.1 %all-to-all-start.1 = ((bf16[8,32,512]{2,1,0:T(8,128)(2,1)}), bf16[8,32,512]{2,1,0:T(8,128)(2,1)S(1)}, u32[]{:S(2)}, u32[]{:S(2)}) async-start(bf16[8,32,512]{2,1,0:T(8,128)(2,1)} %reduce-scatter.2.cloned.1.call-done), calls=%async_computation.2 | async-start | bytes 524288 | tf_op jit(solution)/shard_map/all_to_all | solution.py:123
  128.8 74.8 %all-reduce.6.cloned.1.call-start = ((), (), s32[]{:S(2)}) async-start(), calls=%async_computation.8 | async-start | bytes 524288 | tf_op jit(solution)/shard_map/psum | solution.py:144
Sparse Core Ops, SparseCore 0:
  21.4 34.4 all-reduce.3
  100.3 22.9 reduce-scatter.1
  156.3 31.6 all-reduce.5
Sparse Core Ops, SparseCore 1:
  23.9 59.7 all-gather.5
  102.8 50.4 all-gather.3
  155.2 48.3 all-gather.7
where the time goes:
time: 220 us
  waiting for transfers between devices  123 us (56%)
  blocking collectives  41.7 us (19%)
  matrix products  18.6 us (8%)
  between operations  15.9 us (7%)
  other arithmetic  8.99 us (4%)
  local copies, waits for them, and re-layouts  5.86 us (3%)
  starting transfers between devices  5.78 us (3%)
    all_gather x1, waiting for transfers between devices, on_device(): lax.all_gather(dense_down, 'ep', axis=0, tiled=True)  46.1 us
    all_to_all x1, blocking collectives, on_device(): lax.all_to_all(outgoing, 'ep', split_axis=0, concat_axis=0, tiled=True)  36.1 us
    psum x1, waiting for transfers between devices, on_device(): lax.psum(jnp.dot(gated, proj_out, preferred_element_type=jnp.float32).ast...  33.1 us
    all_gather x1, waiting for transfers between devices, on_device(): lax.all_gather(dense_gate, 'ep', axis=0, tiled=True)  24.4 us
    reduce_scatter x1, waiting for transfers between devices, on_device(): lax.psum_scatter(result.astype(jnp.bfloat16), 'tp', scatter_dimension=2,...  17.5 us
    psum x1, blocking collectives, on_device(): total_square = lax.psum(jnp.sum(combined * combined, axis=1), 'tp')  5.67 us
    all_to_all x1, starting transfers between devices, on_device(): lax.all_to_all(summed, 'ep', split_axis=0, concat_axis=0, tiled=True)  5.53 us
  transfers between devices with their start and end apart: 7, of which 4 were waited for; matrix products, arithmetic and copies ran while one was open for 8% of the time, Pallas kernels for 0%

commit v1 on v0

--- a/solution.py
+++ b/solution.py
@@ -1,6 +1,10 @@
+import functools
+
 import jax
 import jax.numpy as jnp
 from jax import lax
+from jax.experimental import pallas as pl
+from jax.experimental.pallas import tpu as pltpu
 from jax.sharding import PartitionSpec as P
 
 norm_eps = 1e-06
@@ -15,6 +19,464 @@
 def softmax_plain(logits):
     weights = jnp.exp(logits)
     return weights / jnp.sum(weights, axis=-1, keepdims=True)
+
+
+def fused_kernel(
+    ep,
+    group_size,
+    group_count,
+    expert_count,
+    gated_ref,
+    proj_out_ref,
+    resid_ref,
+    post_ref,
+    ffn_ref,
+    router_ref,
+    route_ref,
+    out_gain_ref,
+    gate_hbm,
+    up_hbm,
+    down_hbm,
+    dense_gate_hbm,
+    dense_up_hbm,
+    dense_down_hbm,
+    out_ref,
+    gate_w,
+    up_w,
+    down_w,
+    dgate,
+    dup,
+    ddown,
+    stream_buf,
+    mix_own,
+    mix_peer,
+    half_own,
+    half_far,
+    rows_buf,
+    aux_buf,
+    part_buf,
+    part_peer,
+    send_x,
+    recv_x,
+    send_ep,
+    recv_ep,
+    square_own,
+    square_peer,
+    local_sem,
+    dense_send,
+    dense_recv,
+    mix_send,
+    mix_recv,
+    rows_send,
+    rows_recv,
+    aux_send,
+    aux_recv,
+    forward_send,
+    forward_recv,
+    part_send,
+    part_recv,
+    x_send,
+    x_recv,
+    ep_send,
+    ep_recv,
+    square_send,
+    square_recv,
+):
+    f32, bf16 = jnp.float32, jnp.bfloat16
+    me = lax.axis_index("ep")
+    tp = lax.axis_index("tp")
+    far = tp // 2
+    core = tp % 2
+    beside = far * 2 + (1 - core)
+    across = (1 - far) * 2 + core
+    diagonal = (1 - far) * 2 + (1 - core)
+    near = (beside, across, diagonal)
+    seqs, width = resid_ref.shape
+    quarter = width // 4
+    share = dgate.shape[1]
+
+    def remote(src, dst, send, recv, ep_to, tp_to):
+        return pltpu.make_async_remote_copy(
+            src_ref=src,
+            dst_ref=dst,
+            send_sem=send,
+            recv_sem=recv,
+            device_id=(ep_to, tp_to),
+            device_id_type=pl.DeviceIdType.MESH,
+        )
+
+    def ep_at(step):
+        return lax.rem(me + step + ep, ep)
+
+    local = []
+
+    def load(src, dst):
+        copy = pltpu.make_async_copy(src, dst, local_sem.at[len(local)])
+        copy.start()
+        local.append(copy)
+
+    load(gate_hbm.at[0], gate_w)
+    load(up_hbm.at[0], up_w)
+    for q in range(4):
+        load(down_hbm.at[0, :, pl.ds(q * quarter, quarter)], down_w.at[q])
+    dense_pairs = ((dense_gate_hbm, dgate), (dense_up_hbm, dup), (dense_down_hbm, ddown))
+    for src, dst in dense_pairs:
+        load(src.at[pl.ds(tp * share, share), :], dst.at[tp])
+
+    barrier = pltpu.get_barrier_semaphore()
+    for step in range(1, ep):
+        pl.semaphore_signal(
+            barrier, inc=1, device_id=(ep_at(step), tp), device_id_type=pl.DeviceIdType.MESH
+        )
+    for peer in near:
+        pl.semaphore_signal(
+            barrier, inc=1, device_id=(me, peer), device_id_type=pl.DeviceIdType.MESH
+        )
+
+    mix_own[...] = jnp.dot(
+        gated_ref[...], proj_out_ref[...], preferred_element_type=f32
+    ).astype(bf16)
+    pl.semaphore_wait(barrier, ep - 1 + 3)
+
+    sends = []
+    first = remote(mix_own, mix_peer, mix_send.at[0], mix_recv.at[0], me, beside)
+    first.start()
+    sends.append(first)
+    first.wait_recv()
+    half = width // 2
+    chip_sum = (mix_own[...].astype(f32) + mix_peer[...].astype(f32)).astype(bf16)
+    half_own[0] = chip_sum[:, :half]
+    half_own[1] = chip_sum[:, half:]
+    halves = []
+    for k, peer in enumerate((across, diagonal)):
+        copy = remote(
+            half_own.at[core],
+            half_far.at[core],
+            mix_send.at[1 + k],
+            mix_recv.at[1 + k],
+            me,
+            peer,
+        )
+        copy.start()
+        halves.append(copy)
+    sends += halves
+
+    dense_copies = []
+    for t, (src, dst) in enumerate(dense_pairs):
+        for k, peer in enumerate(near):
+            copy = remote(
+                src.at[pl.ds(peer * share, share), :],
+                dst.at[tp],
+                dense_send.at[3 * t + k],
+                dense_recv.at[3 * t + k],
+                me,
+                peer,
+            )
+            copy.start()
+            dense_copies.append(copy)
+    sends += dense_copies
+    for copy in halves:
+        copy.wait_recv()
+
+    far_sum = jnp.concatenate([half_far[0], half_far[1]], axis=1)
+    mixed = chip_sum.astype(f32) + far_sum.astype(f32)
+    mixed_scale = lax.rsqrt(jnp.mean(mixed * mixed, axis=1, keepdims=True) + norm_eps)
+    stream = (
+        resid_ref[...].astype(f32) + mixed * mixed_scale * post_ref[...].astype(f32)
+    ).astype(bf16)
+    stream_f = stream.astype(f32)
+    feed_scale = lax.rsqrt(jnp.mean(stream_f * stream_f, axis=1, keepdims=True) + norm_eps)
+    feed = (stream_f * feed_scale * ffn_ref[...].astype(f32)).astype(bf16)
+    for q in range(4):
+        rows_buf[q, 0] = feed[:, q * quarter : (q + 1) * quarter]
+        stream_buf[q] = stream[:, q * quarter : (q + 1) * quarter]
+
+    rows_copies = []
+    for step in range(1, ep):
+        copy = remote(
+            rows_buf.at[tp, 0],
+            rows_buf.at[tp, step],
+            rows_send.at[step],
+            rows_recv.at[step],
+            ep_at(step),
+            tp,
+        )
+        copy.start()
+        rows_copies.append(copy)
+    sends += rows_copies
+
+    logits = lax.dot_general(
+        feed, router_ref[...], (((1,), (1,)), ((), ())), preferred_element_type=f32
+    )
+    lane = lax.broadcasted_iota(jnp.int32, logits.shape, 1)
+    route = route_ref[...]
+    picked = lane == route[:, 0:1]
+    for k in range(1, route.shape[1]):
+        picked = picked | (lane == route[:, k : k + 1])
+    weights = jnp.exp(logits)
+    pick = jnp.where(picked, weights, 0.0)
+    group_lane = (lane - expert_count) * group_size
+    in_groups = (lane >= expert_count) & (lane < expert_count + group_count)
+    group = jnp.where(in_groups, weights, 0.0)
+    lead = route[:, 0:1]
+    chosen = in_groups & (lead >= group_lane) & (lead < group_lane + group_size)
+    group_weight = jnp.sum(jnp.where(chosen, weights, 0.0), axis=1, keepdims=True) / jnp.sum(
+        group, axis=1, keepdims=True
+    )
+    pick = pick / jnp.sum(pick, axis=1, keepdims=True) * group_weight
+    switch_lane = expert_count + group_count
+    aux_buf[0] = jnp.where(lane == switch_lane, jax.nn.sigmoid(logits), pick).astype(bf16)
+    aux_copies = []
+    for step in range(1, ep):
+        copy = remote(
+            aux_buf.at[0],
+            aux_buf.at[step],
+            aux_send.at[step],
+            aux_recv.at[step],
+            ep_at(step),
+            tp,
+        )
+        copy.start()
+        aux_copies.append(copy)
+    sends += aux_copies
+
+    to_beside, to_across, to_last = [], [], []
+    for step in range(1, ep):
+        rows_copies[step - 1].wait_recv()
+        for k, (peer, kept) in enumerate(((across, to_across), (beside, to_beside))):
+            copy = remote(
+                rows_buf.at[tp, step],
+                rows_buf.at[tp, step],
+                forward_send.at[k, step],
+                forward_recv.at[k, step],
+                me,
+                peer,
+            )
+            copy.start()
+            kept.append(copy)
+    for step in range(1, ep):
+        to_across[step - 1].wait_recv()
+        copy = remote(
+            rows_buf.at[across, step],
+            rows_buf.at[across, step],
+            forward_send.at[2, step],
+            forward_recv.at[2, step],
+            me,
+            beside,
+        )
+        copy.start()
+        to_last.append(copy)
+    sends += to_across + to_beside + to_last
+    for copy in local:
+        copy.wait()
+    for copy in dense_copies + aux_copies + to_beside + to_last:
+        copy.wait_recv()
+
+    total = ep * seqs
+    gate = up = dense_g = dense_u = None
+    nt = (((1,), (1,)), ((), ()))
+
+    def add(total_sum, value):
+        return value if total_sum is None else total_sum + value
+
+    for q in range(4):
+        rows = rows_buf[q].reshape(total, quarter)
+        span = pl.ds(q * quarter, quarter)
+        gate = add(gate, jnp.dot(rows, gate_w[span, :], preferred_element_type=f32))
+        up = add(up, jnp.dot(rows, up_w[span, :], preferred_element_type=f32))
+        dense_g = add(dense_g, lax.dot_general(rows, dgate[q], nt, preferred_element_type=f32))
+        dense_u = add(dense_u, lax.dot_general(rows, dup[q], nt, preferred_element_type=f32))
+    aux = aux_buf[...].reshape(total, aux_buf.shape[2]).astype(f32)
+    aux_lane = lax.broadcasted_iota(jnp.int32, aux.shape, 1)
+    weight = jnp.sum(jnp.where(aux_lane == me, aux, 0.0), axis=1, keepdims=True)
+    switch = jnp.sum(jnp.where(aux_lane == switch_lane, aux, 0.0), axis=1, keepdims=True)
+    hidden = (gate * jax.nn.sigmoid(gate) * up * weight).astype(bf16)
+    dense_hidden = (dense_g * jax.nn.sigmoid(dense_g) * dense_u * switch).astype(bf16)
+
+    part_copies = []
+    for k, q in enumerate((diagonal, beside, across, tp)):
+        value = jnp.dot(hidden, down_w[q], preferred_element_type=f32) + jnp.dot(
+            dense_hidden, ddown[q], preferred_element_type=f32
+        )
+        part_buf[q] = value.astype(bf16).reshape(ep, seqs, quarter)
+        if k < 2:
+            copy = remote(
+                part_buf.at[q], part_peer.at[k], part_send.at[k], part_recv.at[k], me, beside
+            )
+            copy.start()
+            part_copies.append(copy)
+    sends += part_copies
+
+    order = list(range(1, ep)) + [0]
+    part_copies[0].wait_recv()
+    x_copies = {}
+    for step in order:
+        send_x[step] = (
+            part_buf[across, step].astype(f32) + part_peer[0, step].astype(f32)
+        ).astype(bf16)
+        copy = remote(
+            send_x.at[step], recv_x.at[step], x_send.at[step], x_recv.at[step], me, across
+        )
+        copy.start()
+        x_copies[step] = copy
+        sends.append(copy)
+    part_copies[1].wait_recv()
+    combined = None
+    ep_copies = []
+    for step in order:
+        x_copies[step].wait_recv()
+        value = (
+            part_buf[tp, step].astype(f32)
+            + part_peer[1, step].astype(f32)
+            + recv_x[step].astype(f32)
+        )
+        if step == 0:
+            combined = value
+            continue
+        send_ep[step] = value.astype(bf16)
+        copy = remote(
+            send_ep.at[step],
+            recv_ep.at[step],
+            ep_send.at[step],
+            ep_recv.at[step],
+            ep_at(-step),
+            tp,
+        )
+        copy.start()
+        ep_copies.append(copy)
+    sends += ep_copies
+    for step in range(1, ep):
+        ep_copies[step - 1].wait_recv()
+        combined = combined + recv_ep[step].astype(f32)
+
+    square = jnp.sum(combined * combined, axis=1, keepdims=True)
+    square_own[...] = jnp.broadcast_to(square, square_own.shape)
+    square_copies = []
+    for k, peer in enumerate(near):
+        copy = remote(
+            square_own, square_peer.at[k], square_send.at[k], square_recv.at[k], me, peer
+        )
+        copy.start()
+        square_copies.append(copy)
+    sends += square_copies
+    for copy in square_copies:
+        copy.wait_recv()
+    everything = (square_own[...] + square_peer[0]) + (square_peer[1] + square_peer[2])
+    scale = lax.rsqrt(everything[:, 0:1] / width + norm_eps)
+    own_stream = stream_buf[tp].astype(f32)
+    out_ref[...] = (own_stream + combined * scale * out_gain_ref[...].astype(f32)).astype(bf16)
+    for copy in sends:
+        copy.wait_send()
+
+
+def fused_tail(
+    gated,
+    proj_out,
+    resid,
+    post_gain,
+    ffn_gain,
+    group_router,
+    expert_router,
+    route_experts,
+    expert_gate,
+    expert_up,
+    expert_down,
+    dense_switch,
+    dense_gate,
+    dense_up,
+    dense_down,
+    out_gain,
+):
+    ep = lax.axis_size("ep")
+    seqs, width = resid.shape
+    quarter = width // 4
+    expert_count = expert_router.shape[1]
+    group_count = group_router.shape[1]
+    used = expert_count + group_count + 1
+    lanes = -(-used // 128) * 128
+    router = jnp.concatenate(
+        [
+            expert_router.T,
+            group_router.T,
+            dense_switch[None, :],
+            jnp.zeros((lanes - used, width), expert_router.dtype),
+        ],
+        axis=0,
+    )
+    hidden_here = expert_gate.shape[2]
+    share = dense_gate.shape[0] // 4
+    bf16 = jnp.bfloat16
+    vmem = pl.BlockSpec(memory_space=pltpu.VMEM)
+    hbm = pl.BlockSpec(memory_space=pl.ANY)
+    dma = pltpu.SemaphoreType.DMA
+    kernel = functools.partial(
+        fused_kernel, ep, expert_count // group_count, group_count, expert_count
+    )
+    return pl.pallas_call(
+        kernel,
+        out_shape=jax.ShapeDtypeStruct((seqs, quarter), bf16),
+        in_specs=[vmem] * 8 + [hbm] * 6,
+        out_specs=vmem,
+        scratch_shapes=[
+            pltpu.VMEM((width, hidden_here), bf16),
+            pltpu.VMEM((width, hidden_here), bf16),
+            pltpu.VMEM((4, hidden_here, quarter), bf16),
+            pltpu.VMEM((4, share, quarter), bf16),
+            pltpu.VMEM((4, share, quarter), bf16),
+            pltpu.VMEM((4, share, quarter), bf16),
+            pltpu.VMEM((4, seqs, quarter), bf16),
+            pltpu.VMEM((seqs, width), bf16),
+            pltpu.VMEM((seqs, width), bf16),
+            pltpu.VMEM((2, seqs, width // 2), bf16),
+            pltpu.VMEM((2, seqs, width // 2), bf16),
+            pltpu.VMEM((4, ep, seqs, quarter), bf16),
+            pltpu.VMEM((ep, seqs, lanes), bf16),
+            pltpu.VMEM((4, ep, seqs, quarter), bf16),
+            pltpu.VMEM((2, ep, seqs, quarter), bf16),
+            pltpu.VMEM((ep, seqs, quarter), bf16),
+            pltpu.VMEM((ep, seqs, quarter), bf16),
+            pltpu.VMEM((ep, seqs, quarter), bf16),
+            pltpu.VMEM((ep, seqs, quarter), bf16),
+            pltpu.VMEM((seqs, 128), jnp.float32),
+            pltpu.VMEM((3, seqs, 128), jnp.float32),
+            dma((9,)),
+            dma((9,)),
+            dma((9,)),
+            dma((3,)),
+            dma((3,)),
+            dma((ep,)),
+            dma((ep,)),
+            dma((ep,)),
+            dma((ep,)),
+            dma((3, ep)),
+            dma((3, ep)),
+            dma((2,)),
+            dma((2,)),
+            dma((ep,)),
+            dma((ep,)),
+            dma((ep,)),
+            dma((ep,)),
+            dma((3,)),
+            dma((3,)),
+        ],
+        compiler_params=pltpu.CompilerParams(collective_id=0, has_side_effects=True),
+        name="fused_tail",
+    )(
+        gated,
+        proj_out,
+        resid,
+        post_gain[None, :],
+        ffn_gain[None, :],
+        router,
+        route_experts,
+        out_gain[None, :],
+        expert_gate,
+        expert_up,
+        expert_down,
+        dense_gate,
+        dense_up,
+        dense_down,
+    )
 
 
 def on_device(
@@ -80,6 +542,28 @@
     new_state = keep[:, :, None, None] * scan_state + driven[:, :, :, None] * b_heads[:, :, None, :]
     read = jnp.sum(new_state * c_heads[:, :, None, :], axis=3).reshape(seqs, channels)
     gated = (read * jax.nn.silu(gate_z) * inner_gain.astype(jnp.float32)).astype(jnp.bfloat16)
+    new_conv = history[:, :, 1:, :]
+    whole_blocks = 2 * seqs * route_experts.shape[1] // expert_router.shape[1] >= seqs
+    if whole_blocks and expert_gate.shape[0] == 1 and lax.axis_size("tp") == 4:
+        layer_out = fused_tail(
+            gated,
+            proj_out,
+            resid,
+            post_gain,
+            ffn_gain,
+            group_router,
+            expert_router,
+            route_experts,
+            expert_gate,
+            expert_up,
+            expert_down,
+            dense_switch,
+            dense_gate,
+            dense_up,
+            dense_down,
+            out_gain,
+        )
+        return (layer_out, new_state, new_conv)
     mixed = lax.psum(
         jnp.dot(gated, proj_out, preferred_element_type=jnp.float32).astype(jnp.bfloat16), "tp"
     ).astype(jnp.float32)
@@ -159,7 +643,6 @@
     layer_out = (stream_part + combined * scale[:, None] * out_gain.astype(jnp.float32)).astype(
         jnp.bfloat16
     )
-    new_conv = history[:, :, 1:, :]
     return (layer_out, new_state, new_conv)
 
 

time: 220 us -> 64.7 us (0.29)
  waiting for transfers between devices: 123 us -> 0 us
  Pallas kernels: 0 us -> 46.2 us
  blocking collectives: 41.7 us -> 0 us
  between operations: 15.9 us -> 0.87 us
  matrix products: 18.6 us -> 5.02 us
  starting transfers between devices: 5.78 us -> 0 us
  other arithmetic: 8.99 us -> 5.9 us
    all_gather x3 -> x0, waiting for transfers between devices: 70.5 us -> none  [the longest x1 46.1 us: on_device(): lax.all_gather(dense_down, 'ep', axis=0, tiled=True)]
    pallas_call x0 -> x1, Pallas kernels: none -> 46.2 us  [fused_tail(): pl.pallas_call(kernel, out_shape=jax.ShapeDtypeStruct((seqs, quarter), bf...]
    all_to_all x1 -> x0, blocking collectives: 36.1 us -> none  [on_device(): lax.all_to_all(outgoing, 'ep', split_axis=0, concat_axis=0, tiled=True)]
    psum x2 -> x0, waiting for transfers between devices: 33.1 us -> none  [the longest x1 33.1 us: on_device(): lax.psum(jnp.dot(gated, proj_out, preferred_element_type=jnp.float32).ast...]
    reduce_scatter x1 -> x0, waiting for transfers between devices: 17.5 us -> none  [on_device(): lax.psum_scatter(result.astype(jnp.bfloat16), 'tp', scatter_dimension=2,...]
    dot_general x10 -> x1, matrix products: 13.5 us -> 0.89 us  [on_device(): gate_z = jnp.dot(normed, proj_z, preferred_element_type=jnp.float32)]
    psum x1 -> x0, blocking collectives: 5.67 us -> none  [on_device(): total_square = lax.psum(jnp.sum(combined * combined, axis=1), 'tp')]
    all_to_all x1 -> x0, starting transfers between devices: 5.53 us -> none  [on_device(): lax.all_to_all(summed, 'ep', split_axis=0, concat_axis=0, tiled=True)]
  transfers between devices with their start and end apart: 7 -> 0, of which waited for: 4 -> 0; matrix products, arithmetic and copies ran while one was open for 8% -> 0% of each run, Pallas kernels for 0% -> 0%
where the time goes in v1:
time: 64.7 us; the launch traced here: 64.3 us
  Pallas kernels  46.2 us (71%)
  local copies, waits for them, and re-layouts  6.35 us (10%)
  other arithmetic  5.9 us (9%)
  matrix products  5.02 us (8%)
  between operations  0.87 us (1%)
    pallas_call x1, Pallas kernels, fused_tail(): pl.pallas_call(kernel, out_shape=jax.ShapeDtypeStruct((seqs, quarter), bf...  46.2 us
    unnamed x30, local copies, waits for them, and re-layouts  2.81 us
    reduce_sum x1, other arithmetic, on_device(): jnp.sum(new_state * c_heads[:, :, None, :], axis=3).reshape(seqs, channels)  2.11 us
    dot_general x1, matrix products, on_device(): jnp.dot(normed, proj_b, preferred_element_type=jnp.float32)  1.38 us
    dot_general x1, matrix products, on_device(): jnp.dot(normed, proj_c, preferred_element_type=jnp.float32)  1.38 us

profile of v1, /device:TPU:0, one launch (start us, length us, event | category | flops | bytes accessed | tf_op | source)
XLA Modules:
  0.0 64.3 jit_solution(5354067859493346903)
XLA Ops:
  0.6 0.0 copy-start
  0.6 0.0 copy-start.1
  0.7 0.0 copy-start.10
  0.7 0.0 copy-start.4
  0.7 0.0 copy-start.12
  0.7 0.0 copy-start.13
  0.7 0.0 copy-start.11
  0.7 0.0 copy-start.2
  0.7 0.8 %convert_element_type.30 = f32[2048]{0:T(1024)S(1)} convert(bf16[2048]{0:T(1024)(128)(2,1)} %param.28) | non-fusion elementwise | flops 2048 | bytes 12288 | tf_op jit(solution)/shard_map/convert_element_type | solution.py:16
  1.6 1.1 %fusion.3 = f32[32]{0:T(128)S(1)} fusion(bf16[32,2048]{1,0:T(8,128)(2,1)} %resid_ref.1), kind=kLoop, calls=%fused_computation.11 | loop fusion | flops 196576 | bytes 131200 | tf_op jit(solution)/shard_map/reduce_sum | solution.py:15
  2.7 0.0 copy-done
  2.7 1.2 %fusion = bf16[32,1,1,128]{3,0,2,1:T(8,128)(2,1)S(1)} fusion(bf16[2048,128]{1,0:T(8,128)(2,1)S(1)} %copy-done, bf16[32,2048]{1,0:T(8,128)(2,1)} %resid_ref.1, f32[2048]{0:T(1024)S(1)} %convert_element_type.30, f32[32]{0:T(128)S(1)} %add_rsqrt_fusion), kind=kOutput, calls=%fused_computation.5 | convolution fusion | flops 17043456 | bytes 671872 | tf_op jit(solution)/shard_map/dot_general | solution.py:523
  3.9 1.4 %fusion.1 = bf16[32,1,1,128]{3,0,2,1:T(8,128)(2,1)S(1)} fusion(bf16[2048,128]{1,0:T(8,128)(2,1)} %param.31, bf16[32,2048]{1,0:T(8,128)(2,1)} %resid_ref.1, f32[2048]{0:T(1024)S(1)} %convert_element_type.30, f32[32]{0:T(128)S(1)} %add_rsqrt_fusion), kind=kOutput, calls=%fused_computation.6 | convolution fusion | flops 17043456 | bytes 671872 | tf_op jit(solution)/shard_map/dot_general | solution.py:524
  5.3 1.4 %fusion.2 = bf16[32,1,1,128]{3,0,2,1:T(8,128)(2,1)S(1)} fusion(bf16[2048,128]{1,0:T(8,128)(2,1)} %param.32, bf16[32,2048]{1,0:T(8,128)(2,1)} %resid_ref.1, f32[2048]{0:T(1024)S(1)} %convert_element_type.30, f32[32]{0:T(128)S(1)} %add_rsqrt_fusion), kind=kOutput, calls=%fused_computation.7 | convolution fusion | flops 17043456 | bytes 671872 | tf_op jit(solution)/shard_map/dot_general | solution.py:525
  6.6 0.0 copy-done.10
  6.7 0.0 copy-done.4
  6.8 0.1 reshape_squeeze.3
  6.8 0.0 copy-done.1
  6.9 0.0 copy-done.12
  6.9 0.2 fusion.11
  7.1 0.0 copy-done.13
  7.1 0.0 copy-done.11
  7.1 0.1 multiply_exponential_fusion
  7.2 0.1 copy.31
  7.3 0.1 broadcast_multiply_fusion
  7.4 0.1 copy.30
  7.5 0.0 copy-done.2
  7.5 0.0 copy-start.5
  7.5 0.0 copy-start.6
  7.5 0.0 copy-start.8
  7.5 0.0 copy-start.9
  7.5 2.1 %multiply_reduce_fusion = (f32[32,2,64]{2,1,0:T(2,128)S(1)}, f32[32,2,64,128]{3,2,1,0:T(8,128)}) fusion(f32[32,128]{1,0:T(8,128)S(1)} %get-tuple-element.10, f32[32,128]{1,0:T(8,128)S(1)} %get-tuple-element.11, f32[32,2,64]{2,1,0:T(2,128)S(1)} %broadcast_multiply_fusion, f32[32,2,64,128]{3,2,1,0:T(8,128)S(1)} %copy-done.2, f32[32,2]{1,0:T(8,128)S(1)} %copy.30), kind=kLoop, calls=%fused_computation | loop fusion | flops 2617344 | bytes 4260096 | tf_op jit(solution)/shard_map/reduce_sum | solution.py:543
  9.6 0.1 reshape.79
  9.7 0.7 %convert_element_type.34 = f32[128]{0:T(128)S(1)} convert(bf16[128]{0:T(256)(128)(2,1)} %param.39) | non-fusion elementwise | flops 128 | bytes 768 | tf_op jit(solution)/shard_map/convert_element_type | solution.py:544
  10.4 0.0 copy-done.3
  10.4 0.9 %multiply_convert_fusion.gated_ref = bf16[32,128]{1,0:T(8,128)(2,1)} fusion(f32[32,128]{1,0:T(8,128)S(1)} %reshape.79, f32[128]{0:T(128)S(1)} %convert_element_type.34, bf16[2048,128]{1,0:T(8,128)(2,1)S(1)} %copy-done.3, bf16[32,2048]{1,0:T(8,128)(2,1)S(1)} %copy-done.1, f32[2048]{0:T(1024)S(1)} %convert_element_type.30, f32[32]{0:T(128)S(1)} %add_rsqrt_fusion), kind=kOutput, calls=%fused_computation.19 | convolution fusion | flops 17068032 | bytes 688768 | tf_op jit(solution)/shard_map/dot_general | solution.py:529
  11.3 0.0 copy-done.7
  11.3 0.1 pad.3.clone
  11.4 0.0 copy-done.6
  11.4 0.9 %maximum_maximum_fusion.router_ref = bf16[128,2048]{1,0:T(8,128)(2,1)} fusion(bf16[1,2048]{1,0:T(2,128)(2,1)S(1)} %broadcast_in_dim.12, bf16[2,2048]{1,0:T(2,128)(2,1)S(1)} %bitcast.20, bf16[8,2048]{1,0:T(8,128)(2,1)S(1)} %bitcast.19, bf16[128]{0:T(256)(128)(2,1)S(1)} %pad.3.clone), kind=kLoop, calls=%fused_computation.8 | loop fusion | flops 2097152 | bytes 569600 | tf_op jit(solution)/shard_map/concatenate | solution.py:397
  12.3 1.4 %copy.32.route_ref = s32[32,4]{1,0:T(8,128)} copy(s32[32,4]{0,1:T(4,128)} %param.45) | data formatting | bytes 1024 | tf_op args[18]
  13.7 0.0 copy-done.8
  13.7 0.6 broadcast_in_dim.10.post_ref
  14.3 0.6 broadcast_in_dim.11.ffn_ref
  14.9 1.3 %broadcast_in_dim.14.out_gain_ref = bf16[1,512]{1,0:T(2,128)(2,1)} reshape(bf16[512]{0:T(512)(128)(2,1)} %param.53) | data formatting | bytes 2048 | tf_op jit(solution)/shard_map/broadcast_in_dim | solution.py:472
  16.1 46.2 %fused_tail.1 = bf16[32,512]{1,0:T(8,128)(2,1)} custom-call(bf16[32,128]{1,0:T(8,128)(2,1)} %multiply_convert_fusion.gated_ref, bf16[128,2048]{1,0:T(8,128)(2,1)} %proj_out_ref.1, bf16[32,2048]{1,0:T(8,128)(2,1)} %resid_ref.1, bf16[1,2048]{1,0:T(2,128)(2,1)} %broadcast_in_dim.10.post_ref, bf16[1,2048]{1,0:T(2,128)(2,1)} %broadcast_in_dim.11.ffn_ref, ...), custom_call_target="tpu_custom_call" | custom-call | tf_op jit(solution)/shard_map/fused_tail/pallas_call | solution.py:415
  62.3 0.6 slice.25
  63.0 1.4 %copy.34 = bf16[32,512]{1,0:T(8,128)(2,1)} copy(bf16[32,512]{1,0:T(8,128)(2,1)} %fused_tail.1) | data formatting | bytes 65536
  (12 shorter events, 0.1 us)
Async XLA Ops:
  0.6 2.1 %copy-start = (bf16[2048,128]{1,0:T(8,128)(2,1)S(1)}, bf16[2048,128]{1,0:T(8,128)(2,1)}, u32[]{:S(2)}) copy-start(bf16[2048,128]{1,0:T(8,128)(2,1)} %param.29) | copy-start | bytes 1572868
  0.6 6.2 %copy-start.1 = (bf16[32,2048]{1,0:T(8,128)(2,1)S(1)}, bf16[32,2048]{1,0:T(8,128)(2,1)}, u32[]{:S(2)}) copy-start(bf16[32,2048]{1,0:T(8,128)(2,1)} %resid_ref.1) | copy-start | bytes 393220
  0.7 6.0 %copy-start.10 = (bf16[3,4,128]{2,1,0:T(4,128)(2,1)S(1)}, bf16[3,4,128]{2,1,0:T(4,128)(2,1)}, u32[]{:S(2)}) copy-start(bf16[3,4,128]{2,1,0:T(4,128)(2,1)} %param.36) | copy-start | bytes 9220
  0.7 6.0 %copy-start.4 = (bf16[32,3,3,128]{3,0,2,1:T(8,128)(2,1)S(1)}, bf16[32,3,3,128]{3,0,2,1:T(8,128)(2,1)}, u32[]{:S(2)}) copy-start(bf16[32,3,3,128]{3,0,2,1:T(8,128)(2,1)} %param.37) | copy-start | bytes 221188
  0.7 6.2 %copy-start.12 = (bf16[2048,8]{0,1:T(8,128)(2,1)S(1)}, bf16[2048,8]{0,1:T(8,128)(2,1)}, u32[]{:S(2)}) copy-start(bf16[2048,8]{0,1:T(8,128)(2,1)} %param.33) | copy-start | bytes 98308
  0.7 6.4 %copy-start.13 = (f32[2]{0:T(128)S(1)}, f32[2]{0:T(128)}, u32[]{:S(2)}) copy-start(f32[2]{0:T(128)} %param.35) | copy-start | bytes 28
  0.7 6.4 %copy-start.11 = (f32[2]{0:T(128)S(1)}, f32[2]{0:T(128)}, u32[]{:S(2)}) copy-start(f32[2]{0:T(128)} %param.34) | copy-start | bytes 28
  0.7 6.8 %copy-start.2 = (f32[32,2,64,128]{3,2,1,0:T(8,128)S(1)}, f32[32,2,64,128]{3,2,1,0:T(8,128)}, u32[]{:S(2)}) copy-start(f32[32,2,64,128]{3,2,1,0:T(8,128)} %param.38) | copy-start | bytes 6291460
  7.5 2.9 %copy-start.3 = (bf16[2048,128]{1,0:T(8,128)(2,1)S(1)}, bf16[2048,128]{1,0:T(8,128)(2,1)}, u32[]{:S(2)}) copy-start(bf16[2048,128]{1,0:T(8,128)(2,1)} %param.30) | copy-start | bytes 1572868
  7.5 3.8 %copy-start.7 = (bf16[2048]{0:T(1024)(128)(2,1)S(1)}, bf16[2048]{0:T(1024)(128)(2,1)}, u32[]{:S(2)}) copy-start(bf16[2048]{0:T(1024)(128)(2,1)} %param.49) | copy-start | bytes 12292
  7.5 3.9 %copy-start.5 = (bf16[2048,8]{0,1:T(8,128)(2,1)S(1)}, bf16[2048,8]{0,1:T(8,128)(2,1)}, u32[]{:S(2)}) copy-start(bf16[2048,8]{0,1:T(8,128)(2,1)} %param.44) | copy-start | bytes 98308
  7.5 3.9 %copy-start.6 = (bf16[2048,2]{0,1:T(2,128)(2,1)S(1)}, bf16[2048,2]{0,1:T(2,128)(2,1)}, u32[]{:S(2)}) copy-start(bf16[2048,2]{0,1:T(2,128)(2,1)} %param.43) | copy-start | bytes 24580
  7.5 6.2 %copy-start.8 = (bf16[2048]{0:T(1024)(128)(2,1)S(1)}, bf16[2048]{0:T(1024)(128)(2,1)}, u32[]{:S(2)}) copy-start(bf16[2048]{0:T(1024)(128)(2,1)} %param.41) | copy-start | bytes 12292
  7.5 6.7 %copy-start.9 = (bf16[2048]{0:T(1024)(128)(2,1)S(1)}, bf16[2048]{0:T(1024)(128)(2,1)}, u32[]{:S(2)}) copy-start(bf16[2048]{0:T(1024)(128)(2,1)} %param.42) | copy-start | bytes 12292

commit v2 on v1

--- a/solution.py
+++ b/solution.py
@@ -26,14 +26,27 @@
     group_size,
     group_count,
     expert_count,
-    gated_ref,
     proj_out_ref,
     resid_ref,
+    mix_ref,
     post_ref,
     ffn_ref,
-    router_ref,
+    expert_router_ref,
+    group_router_ref,
+    switch_ref,
     route_ref,
     out_gain_ref,
+    inner_ref,
+    proj_step_ref,
+    taps_ref,
+    conv_ref,
+    bias_ref,
+    decay_ref,
+    proj_x_hbm,
+    proj_z_hbm,
+    proj_b_hbm,
+    proj_c_hbm,
+    state_hbm,
     gate_hbm,
     up_hbm,
     down_hbm,
@@ -41,6 +54,12 @@
     dense_up_hbm,
     dense_down_hbm,
     out_ref,
+    new_state_hbm,
+    new_conv_ref,
+    proj_w,
+    state_buf,
+    new_state_buf,
+    router_buf,
     gate_w,
     up_w,
     down_w,
@@ -63,6 +82,7 @@
     square_own,
     square_peer,
     local_sem,
+    state_sem,
     dense_send,
     dense_recv,
     mix_send,
@@ -115,6 +135,9 @@
         copy.start()
         local.append(copy)
 
+    for k, src in enumerate((proj_x_hbm, proj_b_hbm, proj_c_hbm, proj_z_hbm)):
+        load(src, proj_w.at[k])
+    load(state_hbm, state_buf)
     load(gate_hbm.at[0], gate_w)
     load(up_hbm.at[0], up_w)
     for q in range(4):
@@ -133,12 +156,89 @@
             barrier, inc=1, device_id=(me, peer), device_id_type=pl.DeviceIdType.MESH
         )
 
-    mix_own[...] = jnp.dot(
-        gated_ref[...], proj_out_ref[...], preferred_element_type=f32
-    ).astype(bf16)
+    def row(ref):
+        return ref[...].astype(f32).reshape(1, ref.shape[0])
+
+    resid_f = resid_ref[...].astype(f32)
+    resid_scale = lax.rsqrt(jnp.mean(resid_f * resid_f, axis=1, keepdims=True) + norm_eps)
+    normed = (resid_f * resid_scale * row(mix_ref)).astype(bf16)
+    group_base = -(-expert_count // 8) * 8
+    switch_lane = group_base + -(-group_count // 8) * 8
+    router_buf[...] = jnp.zeros_like(router_buf)
+    router_buf[0:expert_count, :] = expert_router_ref[...].astype(f32)
+    router_buf[group_base : group_base + group_count, :] = group_router_ref[...].astype(f32)
+    router_buf[switch_lane : switch_lane + 1, :] = row(switch_ref)
+    nt = (((1,), (1,)), ((), ()))
+    step_all = lax.dot_general(normed, proj_step_ref[...], nt, preferred_element_type=f32)
     pl.semaphore_wait(barrier, ep - 1 + 3)
 
     sends = []
+    dense_copies = []
+    for t, (src, dst) in enumerate(dense_pairs):
+        for k, peer in enumerate(near):
+            copy = remote(
+                src.at[pl.ds(peer * share, share), :],
+                dst.at[tp],
+                dense_send.at[3 * t + k],
+                dense_recv.at[3 * t + k],
+                me,
+                peer,
+            )
+            copy.start()
+            dense_copies.append(copy)
+    sends += dense_copies
+
+    channels = conv_ref.shape[3]
+    heads = bias_ref.shape[0]
+    head_dim = channels // heads
+    taps = taps_ref[...].astype(f32)
+    old = conv_ref.shape[1]
+    active = []
+    for k in range(3):
+        local[k].wait()
+        fresh = jnp.dot(normed, proj_w[k], preferred_element_type=f32).astype(bf16)
+        summed = conv_ref[k, 0].astype(f32) * taps[k, 0:1]
+        for tap in range(1, old):
+            earlier = conv_ref[k, tap]
+            new_conv_ref[k, tap - 1] = earlier
+            summed = summed + earlier.astype(f32) * taps[k, tap : tap + 1]
+        new_conv_ref[k, old - 1] = fresh
+        summed = summed + fresh.astype(f32) * taps[k, old : old + 1]
+        active.append(summed * jax.nn.sigmoid(summed))
+    inputs, vec_in, vec_read = active
+    local[3].wait()
+    gate_z = jnp.dot(normed, proj_w[3], preferred_element_type=f32)
+    step_lane = lax.broadcasted_iota(jnp.int32, step_all.shape, 1)
+    lane_in = lax.broadcasted_iota(jnp.int32, (seqs, channels), 1)
+    keep = jnp.zeros((seqs, channels), f32)
+    stepped = jnp.zeros((seqs, channels), f32)
+    for h in range(heads):
+        raw = jnp.sum(
+            jnp.where(step_lane == tp * heads + h, step_all, 0.0), axis=1, keepdims=True
+        )
+        raw = raw + bias_ref[h]
+        step = jnp.maximum(raw, 0.0) + jnp.log1p(jnp.exp(-jnp.abs(raw)))
+        mine = (lane_in >= h * head_dim) & (lane_in < (h + 1) * head_dim)
+        keep = jnp.where(mine, jnp.exp(-decay_ref[h] * step), keep)
+        stepped = jnp.where(mine, step, stepped)
+    columns = jnp.concatenate(
+        [keep, stepped * inputs, jnp.zeros((channels - 2 * seqs, channels), f32)], axis=0
+    ).T
+    local[4].wait()
+    read_lane = lax.broadcasted_iota(jnp.int32, (channels, channels), 1)
+    read = jnp.zeros((channels, channels), f32)
+    for t in range(seqs):
+        fresh_state = (
+            columns[:, t : t + 1] * state_buf[t]
+            + columns[:, seqs + t : seqs + t + 1] * vec_in[t : t + 1]
+        )
+        new_state_buf[t] = fresh_state
+        value = jnp.sum(fresh_state * vec_read[t : t + 1], axis=1, keepdims=True)
+        read = jnp.where(read_lane == t, value, read)
+    read = read.T[0:seqs]
+    gated = (read * (gate_z * jax.nn.sigmoid(gate_z)) * row(inner_ref)).astype(bf16)
+    mix_own[...] = jnp.dot(gated, proj_out_ref[...], preferred_element_type=f32).astype(bf16)
+
     first = remote(mix_own, mix_peer, mix_send.at[0], mix_recv.at[0], me, beside)
     first.start()
     sends.append(first)
@@ -161,20 +261,8 @@
         halves.append(copy)
     sends += halves
 
-    dense_copies = []
-    for t, (src, dst) in enumerate(dense_pairs):
-        for k, peer in enumerate(near):
-            copy = remote(
-                src.at[pl.ds(peer * share, share), :],
-                dst.at[tp],
-                dense_send.at[3 * t + k],
-                dense_recv.at[3 * t + k],
-                me,
-                peer,
-            )
-            copy.start()
-            dense_copies.append(copy)
-    sends += dense_copies
+    state_out = pltpu.make_async_copy(new_state_buf, new_state_hbm, state_sem)
+    state_out.start()
     for copy in halves:
         copy.wait_recv()
 
@@ -182,11 +270,11 @@
     mixed = chip_sum.astype(f32) + far_sum.astype(f32)
     mixed_scale = lax.rsqrt(jnp.mean(mixed * mixed, axis=1, keepdims=True) + norm_eps)
     stream = (
-        resid_ref[...].astype(f32) + mixed * mixed_scale * post_ref[...].astype(f32)
+        resid_f + mixed * mixed_scale * row(post_ref)
     ).astype(bf16)
     stream_f = stream.astype(f32)
     feed_scale = lax.rsqrt(jnp.mean(stream_f * stream_f, axis=1, keepdims=True) + norm_eps)
-    feed = (stream_f * feed_scale * ffn_ref[...].astype(f32)).astype(bf16)
+    feed = (stream_f * feed_scale * row(ffn_ref)).astype(bf16)
     for q in range(4):
         rows_buf[q, 0] = feed[:, q * quarter : (q + 1) * quarter]
         stream_buf[q] = stream[:, q * quarter : (q + 1) * quarter]
@@ -206,17 +294,25 @@
     sends += rows_copies
 
     logits = lax.dot_general(
-        feed, router_ref[...], (((1,), (1,)), ((), ())), preferred_element_type=f32
+        feed, router_buf[...].astype(bf16), nt, preferred_element_type=f32
     )
     lane = lax.broadcasted_iota(jnp.int32, logits.shape, 1)
-    route = route_ref[...]
+    same = lax.broadcasted_iota(jnp.int32, (seqs, seqs), 0) == lax.broadcasted_iota(
+        jnp.int32, (seqs, seqs), 1
+    )
+    route = lax.dot_general(
+        jnp.where(same, 1.0, 0.0).astype(bf16),
+        route_ref[...].astype(f32).astype(bf16),
+        nt,
+        preferred_element_type=f32,
+    ).astype(jnp.int32)
     picked = lane == route[:, 0:1]
     for k in range(1, route.shape[1]):
         picked = picked | (lane == route[:, k : k + 1])
     weights = jnp.exp(logits)
     pick = jnp.where(picked, weights, 0.0)
-    group_lane = (lane - expert_count) * group_size
-    in_groups = (lane >= expert_count) & (lane < expert_count + group_count)
+    group_lane = (lane - group_base) * group_size
+    in_groups = (lane >= group_base) & (lane < group_base + group_count)
     group = jnp.where(in_groups, weights, 0.0)
     lead = route[:, 0:1]
     chosen = in_groups & (lead >= group_lane) & (lead < group_lane + group_size)
@@ -224,7 +320,6 @@
         group, axis=1, keepdims=True
     )
     pick = pick / jnp.sum(pick, axis=1, keepdims=True) * group_weight
-    switch_lane = expert_count + group_count
     aux_buf[0] = jnp.where(lane == switch_lane, jax.nn.sigmoid(logits), pick).astype(bf16)
     aux_copies = []
     for step in range(1, ep):
@@ -267,14 +362,13 @@
         copy.start()
         to_last.append(copy)
     sends += to_across + to_beside + to_last
-    for copy in local:
+    for copy in local[5:]:
         copy.wait()
     for copy in dense_copies + aux_copies + to_beside + to_last:
         copy.wait_recv()
 
     total = ep * seqs
     gate = up = dense_g = dense_u = None
-    nt = (((1,), (1,)), ((), ()))
 
     def add(total_sum, value):
         return value if total_sum is None else total_sum + value
@@ -364,15 +458,27 @@
     everything = (square_own[...] + square_peer[0]) + (square_peer[1] + square_peer[2])
     scale = lax.rsqrt(everything[:, 0:1] / width + norm_eps)
     own_stream = stream_buf[tp].astype(f32)
-    out_ref[...] = (own_stream + combined * scale * out_gain_ref[...].astype(f32)).astype(bf16)
+    out_ref[...] = (own_stream + combined * scale * row(out_gain_ref)).astype(bf16)
+    state_out.wait()
     for copy in sends:
         copy.wait_send()
 
 
-def fused_tail(
-    gated,
+def fused_layer(
+    resid,
+    mix_gain,
+    proj_x,
+    proj_z,
+    proj_b,
+    proj_c,
+    proj_step,
+    step_bias,
+    decay_rate,
+    conv_taps,
+    conv_state,
+    scan_state,
+    inner_gain,
     proj_out,
-    resid,
     post_gain,
     ffn_gain,
     group_router,
@@ -390,19 +496,10 @@
     ep = lax.axis_size("ep")
     seqs, width = resid.shape
     quarter = width // 4
+    channels = conv_state.shape[3]
     expert_count = expert_router.shape[1]
     group_count = group_router.shape[1]
-    used = expert_count + group_count + 1
-    lanes = -(-used // 128) * 128
-    router = jnp.concatenate(
-        [
-            expert_router.T,
-            group_router.T,
-            dense_switch[None, :],
-            jnp.zeros((lanes - used, width), expert_router.dtype),
-        ],
-        axis=0,
-    )
+    lanes = 128
     hidden_here = expert_gate.shape[2]
     share = dense_gate.shape[0] // 4
     bf16 = jnp.bfloat16
@@ -412,12 +509,23 @@
     kernel = functools.partial(
         fused_kernel, ep, expert_count // group_count, group_count, expert_count
     )
-    return pl.pallas_call(
+    smem = pl.BlockSpec(memory_space=pltpu.SMEM)
+    earlier = conv_state.transpose(1, 2, 0, 3)
+    state = scan_state.reshape(seqs, channels, scan_state.shape[3])
+    layer_out, new_state, new_conv = pl.pallas_call(
         kernel,
-        out_shape=jax.ShapeDtypeStruct((seqs, quarter), bf16),
-        in_specs=[vmem] * 8 + [hbm] * 6,
-        out_specs=vmem,
+        out_shape=(
+            jax.ShapeDtypeStruct((seqs, quarter), bf16),
+            jax.ShapeDtypeStruct(state.shape, state.dtype),
+            jax.ShapeDtypeStruct(earlier.shape, earlier.dtype),
+        ),
+        in_specs=[vmem] * 14 + [smem] * 2 + [hbm] * 11,
+        out_specs=(vmem, hbm, vmem),
         scratch_shapes=[
+            pltpu.VMEM((4,) + proj_x.shape, bf16),
+            pltpu.VMEM(state.shape, state.dtype),
+            pltpu.VMEM(state.shape, state.dtype),
+            pltpu.VMEM((lanes, width), jnp.float32),
             pltpu.VMEM((width, hidden_here), bf16),
             pltpu.VMEM((width, hidden_here), bf16),
             pltpu.VMEM((4, hidden_here, quarter), bf16),
@@ -439,7 +547,8 @@
             pltpu.VMEM((ep, seqs, quarter), bf16),
             pltpu.VMEM((seqs, 128), jnp.float32),
             pltpu.VMEM((3, seqs, 128), jnp.float32),
-            dma((9,)),
+            dma((14,)),
+            dma,
             dma((9,)),
             dma((9,)),
             dma((3,)),
@@ -460,16 +569,29 @@
             dma((3,)),
         ],
         compiler_params=pltpu.CompilerParams(collective_id=0, has_side_effects=True),
-        name="fused_tail",
+        name="fused_layer",
     )(
-        gated,
         proj_out,
         resid,
-        post_gain[None, :],
-        ffn_gain[None, :],
-        router,
-        route_experts,
-        out_gain[None, :],
+        mix_gain,
+        post_gain,
+        ffn_gain,
+        expert_router.T,
+        group_router.T,
+        dense_switch,
+        route_experts.T,
+        out_gain,
+        inner_gain,
+        proj_step.T,
+        conv_taps,
+        earlier,
+        step_bias,
+        decay_rate,
+        proj_x,
+        proj_z,
+        proj_b,
+        proj_c,
+        state,
         expert_gate,
         expert_up,
         expert_down,
@@ -477,6 +599,7 @@
         dense_up,
         dense_down,
     )
+    return layer_out, new_state.reshape(scan_state.shape), new_conv.transpose(2, 0, 1, 3)
 
 
 def on_device(
@@ -517,6 +640,39 @@
     state_dim = scan_state.shape[3]
     channels = conv_state.shape[3]
     repeat = heads_here // (channels // state_dim)
+    whole_blocks = 2 * seqs * route_experts.shape[1] // expert_router.shape[1] >= seqs
+    one_group = channels == state_dim == 128 and expert_router.shape[1] <= 64
+    few = lax.axis_size("tp") == 4 and expert_gate.shape[0] == 1
+    if whole_blocks and one_group and few:
+        return fused_layer(
+            resid,
+            mix_gain,
+            proj_x,
+            proj_z,
+            proj_b,
+            proj_c,
+            proj_step,
+            step_bias,
+            decay_rate,
+            conv_taps,
+            conv_state,
+            scan_state,
+            inner_gain,
+            proj_out,
+            post_gain,
+            ffn_gain,
+            group_router,
+            expert_router,
+            route_experts,
+            expert_gate,
+            expert_up,
+            expert_down,
+            dense_switch,
+            dense_gate,
+            dense_up,
+            dense_down,
+            out_gain,
+        )
     normed = scaled_rows(resid, mix_gain).astype(jnp.bfloat16)
     fresh = jnp.stack(
         [
@@ -543,27 +699,6 @@
     read = jnp.sum(new_state * c_heads[:, :, None, :], axis=3).reshape(seqs, channels)
     gated = (read * jax.nn.silu(gate_z) * inner_gain.astype(jnp.float32)).astype(jnp.bfloat16)
     new_conv = history[:, :, 1:, :]
-    whole_blocks = 2 * seqs * route_experts.shape[1] // expert_router.shape[1] >= seqs
-    if whole_blocks and expert_gate.shape[0] == 1 and lax.axis_size("tp") == 4:
-        layer_out = fused_tail(
-            gated,
-            proj_out,
-            resid,
-            post_gain,
-            ffn_gain,
-            group_router,
-            expert_router,
-            route_experts,
-            expert_gate,
-            expert_up,
-            expert_down,
-            dense_switch,
-            dense_gate,
-            dense_up,
-            dense_down,
-            out_gain,
-        )
-        return (layer_out, new_state, new_conv)
     mixed = lax.psum(
         jnp.dot(gated, proj_out, preferred_element_type=jnp.float32).astype(jnp.bfloat16), "tp"
     ).astype(jnp.float32)

time: 64.7 us -> 58.8 us (0.909)
  Pallas kernels: 46.2 us -> 52.7 us
  other arithmetic: 5.9 us -> 0 us
  matrix products: 5.02 us -> 0 us
  local copies, waits for them, and re-layouts: 6.35 us -> 5.2 us
    pallas_call x1, Pallas kernels: 46.2 us -> 52.7 us  [fused_layer(): pl.pallas_call(kernel, out_shape=(jax.ShapeDtypeStruct((seqs, quarter), b...]
    dot_general x5 -> x0, matrix products: 5.02 us -> none  [the longest x1 1.38 us: on_device(): jnp.dot(normed, proj_b, preferred_element_type=jnp.float32)]
    reduce_sum x3 -> x0, other arithmetic: 3.26 us -> none  [the longest x1 2.11 us: on_device(): jnp.sum(new_state * c_heads[:, :, None, :], axis=3).reshape(seqs, channels)]
    broadcast_in_dim x5 -> x0, local copies, waits for them, and re-layouts: 2.46 us -> none  [the longest x1 1.25 us: fused_tail(): out_gain[None, :]]
    unnamed x30 -> x5, local copies, waits for them, and re-layouts: 2.81 us -> 5.2 us
    convert_element_type x3 -> x0, other arithmetic: 1.5 us -> none  [the longest x1 0.84 us: scaled_rows(): return values * lax.rsqrt(mean_square + norm_eps) * gain.astype(jnp.float32)]
    concatenate x1 -> x0, other arithmetic: 0.91 us -> none  [fused_tail(): jnp.concatenate([expert_router.T, group_router.T, dense_switch[None, :],...]
where the time goes in v2:
time: 58.8 us; the launch traced here: 58.6 us
  Pallas kernels  52.7 us (90%)
  local copies, waits for them, and re-layouts  5.2 us (9%)
  between operations  0.65 us (1%)
    pallas_call x1, Pallas kernels, fused_layer(): pl.pallas_call(kernel, out_shape=(jax.ShapeDtypeStruct((seqs, quarter), b...  52.7 us
    unnamed x5, local copies, waits for them, and re-layouts  5.2 us

profile of v2, /device:TPU:0, one launch (start us, length us, event | category | flops | bytes accessed | tf_op | source)
XLA Modules:
  0.0 58.6 jit_solution(13465953809454468820)
XLA Ops:
  0.6 52.7 %fused_layer.1 = (bf16[32,512]{1,0:T(8,128)(2,1)}, f32[32,128,128]{2,1,0:T(8,128)}, bf16[3,3,32,128]{3,2,1,0:T(8,128)(2,1)}) custom-call(bf16[128,2048]{1,0:T(8,128)(2,1)} %proj_out_ref.1, bf16[32,2048]{1,0:T(8,128)(2,1)} %resid_ref.1, bf16[2048]{0:T(1024)(128)(2,1)} %mix_ref.1, bf16[2048]{0:T(1024)(128)(2,1)} %post_ref.1, bf16[2048]{0:T(1024)(128)(2,1)} %ffn_ref.1, ...), custom_call_target="tpu_custom_call" | custom-call | tf_op jit(solution)/shard_map/fused_layer/pallas_call | solution.py:515
  53.4 1.4 %copy.33 = bf16[32,512]{1,0:T(8,128)(2,1)} copy(bf16[32,512]{1,0:T(8,128)(2,1)} %get-tuple-element.12) | data formatting | bytes 65536
  54.7 0.0 copy-start
  54.7 3.2 %copy.34 = f32[32,2,64,128]{3,2,1,0:T(8,128)} copy(f32[32,2,64,128]{3,2,1,0:T(8,128)} %bitcast.9) | data formatting | bytes 4194304
  57.9 0.0 copy-done
  57.9 0.6 %copy.35 = bf16[32,3,3,128]{3,0,2,1:T(8,128)(2,1)} copy(bf16[32,3,3,128]{3,0,2,1:T(8,128)(2,1)S(1)} %bitcast.11) | data formatting | bytes 147456
Async XLA Ops:
  54.7 3.2 %copy-start = (bf16[3,3,32,128]{3,2,1,0:T(8,128)(2,1)S(1)}, bf16[3,3,32,128]{3,2,1,0:T(8,128)(2,1)}, u32[]{:S(2)}) copy-start(bf16[3,3,32,128]{3,2,1,0:T(8,128)(2,1)} %get-tuple-element.8) | copy-start | bytes 221188
